TPU v7x, 1024 devices: a 2x16x16 block of a 4x16x16 slice. The times are simulated.
1024 devices in a mesh: grp: 2 (over x), tp: 16 (over z), dp: 32 (over y, core).
Axes of the slice: x: 2, y: 16, z: 16, core: 2. Of those that a mesh axis runs over, the one named last changes fastest.
The devices are a block of a 4x16x16 slice.
Arguments:
- stream: bfloat16 [256, 4096], P('grp', 'dp'), parts along dimension 0, may hold values from -11 to 11
- states: float32 [2, 256, 32, 64, 64], P(None, ('grp', 'dp'), 'tp'), parts along dimension 1, may hold values from -6 to 6
- norm_gain: bfloat16 [2, 4096], P(None, 'dp'), may hold values from 0.099609375 to 1.8984375
- recept_weight: bfloat16 [2, 4096, 2048], P(None, 'dp', 'tp'), may hold values from -0.09375 to 0.09375
- key_weight: bfloat16 [2, 4096, 2048], P(None, 'dp', 'tp'), may hold values from -0.09375 to 0.09375
- value_weight: bfloat16 [2, 4096, 2048], P(None, 'dp', 'tp'), may hold values from -0.09375 to 0.09375
- decay_weight: bfloat16 [2, 4096, 2048], P(None, 'dp', 'tp'), may hold values from -0.09375 to 0.09375
- rate_weight: bfloat16 [2, 4096, 2048], P(None, 'dp', 'tp'), may hold values from -0.09375 to 0.09375
- gate_weight: bfloat16 [2, 4096, 2048], P(None, 'dp', 'tp'), may hold values from -0.09375 to 0.09375
- out_weight: bfloat16 [2, 2048, 4096], P(None, 'tp', 'dp'), may hold values from -0.125 to 0.125
- decay_bias: float32 [2, 2048], P(None, 'tp'), may hold values from -2 to 2
- head_gain: bfloat16 [2, 2048], P(None, 'tp'), may hold values from 0.099609375 to 1.8984375
Outputs:
- new_stream: bfloat16 [256, 4096], P('grp', 'dp'), parts along dimension 0
- new_states: float32 [2, 256, 32, 64, 64], P(None, ('grp', 'dp'), 'tp'), parts along dimension 1
There are 2 independent parts, one for each index of `grp`. A program takes and returns all parts, laid end to end along the dimension named above; an argument that names none is the same for every part. Nothing has to cross between parts.
All inputs are finite; a program needn't handle non-finite values.
Results may differ from a plain program's by a relative error of at most 0.0068.
Values may be sent and summed in bfloat16 or wider, within the bound.
A program may use at most 32 MiB of HBM per device.

v0:
```python
import math

import jax
import jax.numpy as jnp
from jax import lax
from jax.sharding import PartitionSpec as P

D = 4096
HEAD = 64


def in_blocks(x, dim, size):
    before, after = (x.shape[:dim], x.shape[dim + 1 :])
    return jnp.moveaxis(x.reshape(*before, size, -1, *after), dim, 0)


def summed_on_arrival(x, axis, dim):
    size = lax.axis_size(axis)
    pieces = lax.all_to_all(in_blocks(x, dim, size), axis, 0, 0, tiled=True)
    return jnp.sum(pieces, axis=0)


def sent_together(arrays, axis, dim, along):
    widths = [math.prod(a.shape[along:]) for a in arrays]
    both = jnp.concatenate(
        [a.reshape(*a.shape[:along], w) for a, w in zip(arrays, widths)], axis=along
    )
    out = summed_on_arrival(both, axis, dim)
    pieces = jnp.split(out, [sum(widths[:k]) for k in range(1, len(widths))], axis=along)
    return tuple((b.reshape(*out.shape[:along], *a.shape[along:]) for a, b in zip(arrays, pieces)))


def joined_along(pieces, dim):
    pieces = jnp.moveaxis(pieces, 0, dim)
    lengths = pieces.shape
    return pieces.reshape(*lengths[:dim], lengths[dim] * lengths[dim + 1], *lengths[dim + 2 :])


def from_everyone(x, axis):
    copies = jnp.broadcast_to(x, (lax.axis_size(axis), *x.shape))
    return lax.all_to_all(copies, axis, split_axis=0, concat_axis=0, tiled=True)


def gathered_copies(x, axis, dim):
    return joined_along(from_everyone(x, axis), dim)


def over_copies(x, axis):
    everything = from_everyone(x, axis)
    return jnp.sum(everything, axis=0)


def run_block(stream, state_blk, gain, weights, out_weight, bias, hgain):
    current = stream.astype(jnp.float32)
    squares = jnp.sum(current * current, axis=1)
    normed = (current * gain.astype(jnp.float32)).astype(jnp.bfloat16)
    width = weights[0].shape[1]
    local_rows = state_blk.shape[0]
    summed, totals = sent_together(
        (
            jnp.concatenate(
                [jnp.dot(normed, weight, preferred_element_type=jnp.float32) for weight in weights],
                axis=1,
            ),
            squares,
        ),
        "dp",
        0,
        1,
    )
    inv_rms = lax.rsqrt(totals / D + 1e-06)[:, None]
    projected = (summed * inv_rms).reshape(local_rows, 6, -1, HEAD)
    recept = projected[:, 0]
    key_vec = projected[:, 1]
    value_vec = projected[:, 2]
    decay_pre = projected[:, 3]
    rate_pre = projected[:, 4]
    gate_pre = projected[:, 5]
    unit_key = key_vec * lax.rsqrt(jnp.sum(key_vec * key_vec, axis=2, keepdims=True) + 1e-06)
    rate_vec = jax.nn.sigmoid(rate_pre)
    decay = jnp.exp(-0.606531 * jax.nn.sigmoid(bias.reshape(1, -1, HEAD) + decay_pre))
    removed = jnp.einsum("bhij,bhj->bhi", state_blk, unit_key, precision=lax.Precision.HIGHEST)
    new_state = (
        state_blk * decay[:, :, None, :]
        - removed[..., None] * (unit_key * rate_vec)[:, :, None, :]
        + value_vec[..., None] * key_vec[:, :, None, :]
    )
    read = jnp.einsum("bhij,bhj->bhi", new_state, recept, precision=lax.Precision.HIGHEST)
    center = read - jnp.mean(read, axis=2, keepdims=True)
    normal_read = center * lax.rsqrt(jnp.mean(center * center, axis=2, keepdims=True) + 1e-05)
    gated = normal_read * hgain.astype(jnp.float32).reshape(1, -1, HEAD) * jax.nn.sigmoid(gate_pre)
    mixed = gated.reshape(local_rows, width).astype(jnp.bfloat16)
    branch_part = jnp.dot(
        gathered_copies(mixed, "dp", 0), out_weight, preferred_element_type=jnp.float32
    )
    branch = over_copies(branch_part, "tp")
    return ((current + branch).astype(jnp.bfloat16), new_state)


def per_device(
    stream,
    states,
    norm_gain,
    recept_weight,
    key_weight,
    value_weight,
    decay_weight,
    rate_weight,
    gate_weight,
    out_weight,
    decay_bias,
    head_gain,
):
    current = stream
    fresh_list = []
    for layer in range(2):
        weights = (
            recept_weight[layer],
            key_weight[layer],
            value_weight[layer],
            decay_weight[layer],
            rate_weight[layer],
            gate_weight[layer],
        )
        current, fresh = run_block(
            current,
            states[layer],
            norm_gain[layer],
            weights,
            out_weight[layer],
            decay_bias[layer],
            head_gain[layer],
        )
        fresh_list.append(fresh)
    return (current, jnp.stack(fresh_list))


def solution(mesh):
    in_specs = (
        P("grp", "dp"),
        P(None, ("grp", "dp"), "tp", None, None),
        P(None, "dp"),
        P(None, "dp", "tp"),
        P(None, "dp", "tp"),
        P(None, "dp", "tp"),
        P(None, "dp", "tp"),
        P(None, "dp", "tp"),
        P(None, "dp", "tp"),
        P(None, "tp", "dp"),
        P(None, "tp"),
        P(None, "tp"),
    )
    out_specs = (P("grp", "dp"), P(None, ("grp", "dp"), "tp", None, None))
    return jax.shard_map(
        per_device, mesh=mesh, in_specs=in_specs, out_specs=out_specs, check_vma=False
    )
```

profile of v0, /device:TPU:5, one launch (start us, length us, event | category | flops | bytes accessed | tf_op | source)
XLA Modules:
  0.0 316.1 jit_solution(6494616141291658128)
XLA Ops:
  0.6 0.7 bitcast_convert_fusion
  1.4 0.9 fusion.31
  2.3 0.3 copy.110
  2.7 0.4 copy-done.2
  3.2 0.7 copy-done.3
  4.0 0.7 copy-done.4
  4.9 0.7 copy-done.5
  5.7 0.7 copy-done.6
  6.6 0.7 copy-done.7
  7.4 1.1 copy.111
  8.5 87.4 %all-to-all-start = ((f32[32,4,769]{2,1,0:T(4,128)}), f32[32,4,769]{2,1,0:T(4,128)S(1)}, u32[]{:S(2)}, u32[]{:S(2)}) async-start(f32[32,4,769]{2,1,0:T(4,128)} %copy.111), calls=%async_computation | async-start | bytes 917504 | tf_op jit(solution)/shard_map/all_to_all | solution.py:19
  96.1 30.1 %all-to-all-done = f32[32,4,769]{2,1,0:T(4,128)S(1)} async-done(((f32[32,4,769]{2,1,0:T(4,128)}), f32[32,4,769]{2,1,0:T(4,128)S(1)}, u32[]{:S(2)}, u32[]{:S(2)}) %all-to-all-start) | async-done | bytes 393760 | tf_op jit(solution)/shard_map/all_to_all | solution.py:19
  126.8 0.5 fusion.6
  127.3 0.7 fusion.10
  128.1 0.2 multiply_reduce_fusion.2
  128.5 16.0 %all_to_all.30 = bf16[32,4,128]{2,1,0:T(4,128)(2,1)S(1)} all-to-all(bf16[32,4,128]{2,1,0:T(4,128)(2,1)S(1)} %broadcast_in_dim.8), channel_id=1, replica_groups=mesh['grp'=2,'tp'=16,'dp'=32] {'dp'}, dimensions={0} | all-to-all | bytes 65536 | tf_op jit(solution)/shard_map/all_to_all | solution.py:41
  144.7 56.2 %all_to_all.31 = f32[16,128,128]{2,1,0:T(8,128)S(1)} all-to-all(f32[16,128,128]{2,1,0:T(8,128)S(1)} %broadcast_in_dim.9), channel_id=1, replica_groups=mesh['grp'=2,'tp'=16,'dp'=32] {'tp'}, dimensions={0} | all-to-all | bytes 2097152 | tf_op jit(solution)/shard_map/all_to_all | solution.py:41
  201.0 0.7 copy-done.1
  202.7 0.3 copy.121
  203.1 1.1 copy.122
  204.2 10.7 %all-to-all-start.3 = ((f32[32,4,769]{2,1,0:T(4,128)}), f32[32,4,769]{2,1,0:T(4,128)S(1)}, u32[]{:S(2)}, u32[]{:S(2)}) async-start(f32[32,4,769]{2,1,0:T(4,128)} %copy.122), calls=%async_computation.3 | async-start | bytes 917504 | tf_op jit(solution)/shard_map/all_to_all | solution.py:19
  215.0 30.2 %all-to-all-done.3 = f32[32,4,769]{2,1,0:T(4,128)S(1)} async-done(((f32[32,4,769]{2,1,0:T(4,128)}), f32[32,4,769]{2,1,0:T(4,128)S(1)}, u32[]{:S(2)}, u32[]{:S(2)}) %all-to-all-start.3) | async-done | bytes 393760 | tf_op jit(solution)/shard_map/all_to_all | solution.py:19
  245.7 0.5 fusion
  246.3 0.7 fusion.4
  247.0 0.2 multiply_reduce_fusion
  247.4 16.0 %all_to_all.32 = bf16[32,4,128]{2,1,0:T(4,128)(2,1)S(1)} all-to-all(bf16[32,4,128]{2,1,0:T(4,128)(2,1)S(1)} %broadcast_in_dim.10), channel_id=1, replica_groups=mesh['grp'=2,'tp'=16,'dp'=32] {'dp'}, dimensions={0} | all-to-all | bytes 65536 | tf_op jit(solution)/shard_map/all_to_all | solution.py:41
  263.6 1.1 broadcast_in_dim.11
  264.7 6.4 %all-to-all-start.5 = ((f32[16,128,128]{2,1,0:T(8,128)}), f32[16,128,128]{2,1,0:T(8,128)S(1)}, u32[]{:S(2)}, u32[]{:S(2)}) async-start(f32[16,128,128]{2,1,0:T(8,128)} %broadcast_in_dim.11), calls=%async_computation.5 | async-start | bytes 2097152 | tf_op jit(solution)/shard_map/all_to_all | solution.py:41
  271.0 0.3 multiply_add_fusion.1
  271.4 0.8 pad_maximum_fusion
  272.2 43.2 %all-to-all-done.5 = f32[16,128,128]{2,1,0:T(8,128)S(1)} async-done(((f32[16,128,128]{2,1,0:T(8,128)}), f32[16,128,128]{2,1,0:T(8,128)S(1)}, u32[]{:S(2)}, u32[]{:S(2)}) %all-to-all-start.5) | async-done | bytes 1048608 | tf_op jit(solution)/shard_map/all_to_all | solution.py:41
  315.5 0.6 fusion.35
  (71 shorter events, 4.5 us)
Async XLA Ops:
  2.2 0.8 copy-start.2
  3.1 0.8 copy-start.3
  3.9 0.8 copy-start.4
  4.8 0.8 copy-start.5
  5.6 0.8 copy-start.6
  6.4 0.8 copy-start.7
  8.5 87.4 %copy-start.9 = (bf16[2,128]{1,0:T(2,128)(2,1)S(1)}, bf16[2,128]{1,0:T(2,128)(2,1)}, u32[]{:S(2)}) copy-start(bf16[2,128]{1,0:T(2,128)(2,1)} %param.23) | copy-start | bytes 1540
  8.5 87.4 %copy-start.10 = (f32[2,128]{1,0:T(2,128)S(1)}, f32[2,128]{1,0:T(2,128)}, u32[]{:S(2)}) copy-start(f32[2,128]{1,0:T(2,128)} %param.22) | copy-start | bytes 3076
  8.5 117.7 %all-to-all-start = ((f32[32,4,769]{2,1,0:T(4,128)}), f32[32,4,769]{2,1,0:T(4,128)S(1)}, u32[]{:S(2)}, u32[]{:S(2)}) async-start(f32[32,4,769]{2,1,0:T(4,128)} %copy.111), calls=%async_computation | async-start | bytes 917504 | tf_op jit(solution)/shard_map/all_to_all | solution.py:19
  95.9 30.9 %copy-start = (f32[2,4,2,64,64]{4,3,2,1,0:T(8,128)S(1)}, f32[2,4,2,64,64]{4,3,2,1,0:T(8,128)}, u32[]{:S(2)}) copy-start(f32[2,4,2,64,64]{4,3,2,1,0:T(8,128)} %param.13) | copy-start | bytes 786436
  128.1 16.4 %copy-start.8 = (bf16[2,128,128]{2,1,0:T(8,128)(2,1)S(1)}, bf16[2,128,128]{2,1,0:T(8,128)(2,1)}, u32[]{:S(2)}) copy-start(bf16[2,128,128]{2,1,0:T(8,128)(2,1)} %param.21) | copy-start | bytes 196612
  200.9 0.8 copy-start.1
  204.2 41.0 %all-to-all-start.3 = ((f32[32,4,769]{2,1,0:T(4,128)}), f32[32,4,769]{2,1,0:T(4,128)S(1)}, u32[]{:S(2)}, u32[]{:S(2)}) async-start(f32[32,4,769]{2,1,0:T(4,128)} %copy.122), calls=%async_computation.3 | async-start | bytes 917504 | tf_op jit(solution)/shard_map/all_to_all | solution.py:19
  264.7 50.8 %all-to-all-start.5 = ((f32[16,128,128]{2,1,0:T(8,128)}), f32[16,128,128]{2,1,0:T(8,128)S(1)}, u32[]{:S(2)}, u32[]{:S(2)}) async-start(f32[16,128,128]{2,1,0:T(8,128)} %broadcast_in_dim.11), calls=%async_computation.5 | async-start | bytes 2097152 | tf_op jit(solution)/shard_map/all_to_all | solution.py:41
where the time goes:
time: 322 us; the launch traced here: 316 us
  starting transfers between devices  104 us (32%)
  waiting for transfers between devices  104 us (32%)
  blocking collectives  88.2 us (27%)
  local copies, waits for them, and re-layouts  9.64 us (3%)
  other arithmetic  5.28 us (2%)
  matrix products  4.21 us (1%)
    all_to_all x2, starting transfers between devices, summed_on_arrival(): pieces = lax.all_to_all(in_blocks(x, dim, size), axis, 0, 0, tiled=True)  98 us
    all_to_all x3, blocking collectives, from_everyone(): return lax.all_to_all(copies, axis, split_axis=0, concat_axis=0, tiled=True)  88.2 us
    all_to_all x2, waiting for transfers between devices, summed_on_arrival(): pieces = lax.all_to_all(in_blocks(x, dim, size), axis, 0, 0, tiled=True)  60.3 us
    all_to_all x1, waiting for transfers between devices, from_everyone(): return lax.all_to_all(copies, axis, split_axis=0, concat_axis=0, tiled=True)  43.2 us
  transfers between devices with their start and end apart: 3, of which 3 were waited for; matrix products, arithmetic and copies ran while one was open for 0% of the time, Pallas kernels for 0%

commit v1 on v0

v1 whole, which is shorter than its diff:
```python
import functools

import jax
import jax.numpy as jnp
from jax import lax
from jax.experimental import pallas as pl
from jax.experimental.pallas import tpu as pltpu
from jax.sharding import PartitionSpec as P

HEAD = 64
LANES = 128
MESH = pl.DeviceIdType.MESH
F32 = jnp.float32
BF16 = jnp.bfloat16


def rows_of(shape):
    return lax.broadcasted_iota(jnp.int32, shape, 0)


def mix(a, b):
    n = a.shape[0]
    low = (rows_of(a.shape) & 4) == 0
    return (
        jnp.where(low, a, pltpu.roll(b, 4, 0)),
        jnp.where(low, pltpu.roll(a, n - 4, 0), b),
    )


def per_head_sum(t):
    first = lax.broadcasted_iota(jnp.int32, t.shape, 1) < HEAD
    s0 = jnp.sum(jnp.where(first, t, 0.0), axis=1, keepdims=True)
    s1 = jnp.sum(jnp.where(first, 0.0, t), axis=1, keepdims=True)
    return jnp.where(first, s0, s1)


def sigmoid(t):
    return 1.0 / (1.0 + jnp.exp(-t))


def kernel(
    ny,
    nz,
    model,
    stream,
    states,
    gain,
    w0,
    w1,
    w2,
    w3,
    w4,
    w5,
    wout,
    bias,
    hgain,
    out_x,
    out_s,
    xin,
    gbuf,
    wbuf,
    obuf,
    bbuf,
    hbuf,
    sbuf,
    nbuf,
    sy,
    ry,
    my,
    xm,
    sz,
    rz,
    az,
    fx,
    ox,
    load_sem,
    part_send,
    part_recv,
    send_sem,
    recv_sem,
    store_sem,
):
    z = lax.axis_index("tp")
    d = lax.axis_index("dp")
    y = d // 2
    c = lax.rem(d, 2)
    half = 4 * ny

    def y_peer(k):
        return {"dp": lax.rem(y + k, ny) * 2 + c}

    def z_peer(k):
        return {"tp": lax.rem(z + k, nz)}

    partner = {"dp": 2 * y + 1 - c}

    barrier = pltpu.get_barrier_semaphore()

    def greet(n, peer):
        def body(k, carry):
            pl.semaphore_signal(barrier, inc=1, device_id=peer(k), device_id_type=MESH)
            return carry

        lax.fori_loop(1, n, body, 0)

    pl.semaphore_signal(barrier, inc=1, device_id=partner, device_id_type=MESH)
    greet(ny, y_peer)
    greet(nz, z_peer)

    weights = (w0, w1, w2, w3, w4, w5)
    loads = {}

    def load(name, src, dst, k):
        copy = pltpu.make_async_copy(src, dst, load_sem.at[k])
        copy.start()
        loads[name] = copy

    load("x", stream, xin.at[c], 0)
    load("g", gain, gbuf.at[c], 1)
    for r in range(6):
        load(f"w0{r}", weights[r].at[0], wbuf.at[0, c, :, pl.ds(r * LANES, LANES)], 2 + r)
    load("b", bias, bbuf, 8)
    load("h", hgain, hbuf, 9)
    load("s", states, sbuf, 10)
    load("o", wout, obuf.at[c], 11)
    for r in range(6):
        load(f"w1{r}", weights[r].at[1], wbuf.at[1, c, :, pl.ds(r * LANES, LANES)], 12 + r)

    def exchange(src, dst, k):
        return pltpu.make_async_remote_copy(
            src_ref=src,
            dst_ref=dst,
            send_sem=part_send.at[k],
            recv_sem=part_recv.at[k],
            device_id=partner,
            device_id_type=MESH,
        )

    swaps = [
        exchange(xin.at[c], xin.at[c], 0),
        exchange(gbuf.at[c], gbuf.at[c], 1),
        exchange(wbuf.at[0, c], wbuf.at[0, c], 2),
        exchange(obuf.at[c], obuf.at[c], 3),
        exchange(wbuf.at[1, c], wbuf.at[1, c], 4),
        exchange(fx.at[0], fx.at[1], 5),
    ]

    def send_all(n, peer, here, src, dst, k):
        def body(i, carry):
            h = (i + 1) // 2
            off = n // 2 + h * (1 - 2 * lax.rem(i, 2))
            target = lax.rem(here + off, n)
            pltpu.make_async_remote_copy(
                src_ref=src(target),
                dst_ref=dst(n - off),
                send_sem=send_sem.at[k],
                recv_sem=recv_sem.at[k],
                device_id=peer(off),
                device_id_type=MESH,
            ).start()
            return carry

        lax.fori_loop(0, n - 1, body, 0)

    def wait_all(ref, sem):
        pltpu.make_async_copy(ref, ref, sem).wait()

    loads["x"].wait()
    loads["g"].wait()
    for r in range(6):
        loads[f"w0{r}"].wait()
    pl.semaphore_wait(barrier, ny + nz - 1)
    for k in range(3):
        swaps[k].start()
    loads["o"].wait()
    swaps[3].start()
    for r in range(6):
        loads[f"w1{r}"].wait()
    swaps[4].start()
    for k in range(2):
        swaps[k].wait()

    parts = []
    for core in range(2):
        x = xin[core].astype(F32).reshape(ny // 2, 2, 8, LANES)
        p0, p1 = mix(x[:, 0].reshape(half, LANES), x[:, 1].reshape(half, LANES))
        parts.append(jnp.where(c == 0, p0, p1))

    for layer in range(2):
        y_base = 4 * layer
        even, odd = mix(parts[0], parts[1])
        xm[layer, :, 0] = even.reshape(ny // 2, 8, LANES)
        xm[layer, :, 1] = odd.reshape(ny // 2, 8, LANES)

        normed = jnp.concatenate(
            [parts[core] * gbuf[core, layer : layer + 1].astype(F32) for core in range(2)], axis=1
        ).astype(BF16)
        squares = jnp.sum(parts[0] * parts[0] + parts[1] * parts[1], axis=1, keepdims=True)
        squares = jnp.broadcast_to(squares, (half, LANES))
        coarse = squares.astype(BF16).astype(F32)
        fine = squares - coarse
        if layer == 0:
            swaps[2].wait()
        else:
            swaps[4].wait()
        proj = jnp.dot(
            normed, wbuf[layer].reshape(2 * LANES, 6 * LANES), preferred_element_type=F32
        )
        even, odd = mix(
            jnp.concatenate([proj[:, : 3 * LANES], coarse], axis=1),
            jnp.concatenate([proj[:, 3 * LANES :], fine], axis=1),
        )
        sy[layer, :, 0] = even.reshape(ny // 2, 8, 4 * LANES).astype(BF16)
        sy[layer, :, 1] = odd.reshape(ny // 2, 8, 4 * LANES).astype(BF16)
        send_all(
            ny,
            y_peer,
            y,
            lambda t: sy.at[layer, t // 2, lax.rem(t, 2)],
            lambda slot: ry.at[layer, slot],
            y_base,
        )
        if layer == 0:
            loads["b"].wait()
            loads["h"].wait()
            loads["s"].wait()
        total = sy[layer, y // 2, lax.rem(y, 2)].astype(F32)
        wait_all(ry.at[layer, pl.ds(1, ny - 1)], recv_sem.at[y_base])
        for k in range(1, ny):
            total = total + ry[layer, k].astype(F32)

        sq = total[:, 3 * LANES :]
        inv_rms = lax.rsqrt((sq + pltpu.roll(sq, 4, 0)) * (1.0 / model) + 1e-06)
        pr = total[:, : 3 * LANES] * jnp.concatenate([inv_rms] * 3, axis=1)
        lower = pltpu.roll(pr, 4, 0)
        recept, key_vec, value_vec = (pr[:, k * LANES : (k + 1) * LANES] for k in range(3))
        decay_pre, rate_pre, gate_pre = (lower[:, k * LANES : (k + 1) * LANES] for k in range(3))
        unit_key = key_vec * lax.rsqrt(per_head_sum(key_vec * key_vec) + 1e-06)
        key_rate = unit_key * sigmoid(rate_pre)
        decay = jnp.exp(-0.606531 * sigmoid(bbuf[layer : layer + 1] + decay_pre))
        decay_recept = decay * recept
        lhs = jnp.concatenate(
            [
                unit_key[:, :HEAD],
                unit_key[:, HEAD:],
                decay_recept[:, :HEAD],
                decay_recept[:, HEAD:],
            ],
            axis=0,
        )
        found = lax.dot_general(
            lhs,
            sbuf[layer].reshape(8 * HEAD, HEAD),
            (((1,), (1,)), ((), ())),
            precision=lax.Precision.HIGHEST,
            preferred_element_type=F32,
        )
        row = rows_of((8, LANES))
        first = lax.broadcasted_iota(jnp.int32, (8, LANES), 1) < HEAD
        removed = jnp.zeros((8, LANES), F32)
        kept = jnp.zeros((8, LANES), F32)
        for s in range(4):
            blk = found[:, s * LANES : (s + 1) * LANES]
            removed = jnp.where(row == s, jnp.where(first, blk[0:8], blk[8:16]), removed)
            kept = jnp.where(row == s, jnp.where(first, blk[16:24], blk[24:32]), kept)
        read = (
            kept
            - removed * per_head_sum(key_rate * recept)
            + value_vec * per_head_sum(key_vec * recept)
        )
        center = read - per_head_sum(read) * (1.0 / HEAD)
        var = per_head_sum(center * center) * (1.0 / HEAD)
        gated = (
            center
            * lax.rsqrt(var + 1e-05)
            * hbuf[layer : layer + 1].astype(F32)
            * sigmoid(gate_pre)
        )
        gated = jnp.where(row < 4, gated, 0.0)
        gated = jnp.where(lax.rem(y, 2) == 0, gated, pltpu.roll(gated, 4, 0))
        my[layer, y // 2, lax.rem(y, 2)] = gated.astype(BF16)
        mine_y = my.at[layer, y // 2, lax.rem(y, 2)]
        send_all(ny, y_peer, y, lambda t: mine_y, lambda slot: mine_y, y_base + 1)

        removed_t = jnp.transpose(removed)
        value_t = jnp.transpose(value_vec)
        for h in range(2):
            lanes = slice(h * HEAD, (h + 1) * HEAD)
            dec_h, kr_h, key_h = decay[:, lanes], key_rate[:, lanes], key_vec[:, lanes]
            for s in range(4):
                nbuf[layer, s, h] = (
                    sbuf[layer, s, h] * dec_h[s : s + 1]
                    - removed_t[lanes, s : s + 1] * kr_h[s : s + 1]
                    + value_t[lanes, s : s + 1] * key_h[s : s + 1]
                )
        store = pltpu.make_async_copy(nbuf.at[layer], out_s.at[layer], store_sem.at[layer])
        store.start()

        if layer == 0:
            swaps[3].wait()
        wait_all(ry.at[layer, pl.ds(1, ny - 1), :, pl.ds(0, LANES)], recv_sem.at[y_base + 1])
        gathered = (my[layer, :, 0] + my[layer, :, 1]).astype(F32)
        mixed = gathered.reshape(half, LANES).astype(BF16)
        even, odd = mix(
            jnp.dot(mixed, obuf[0, layer], preferred_element_type=F32),
            jnp.dot(mixed, obuf[1, layer], preferred_element_type=F32),
        )
        sz[layer, :, 0] = even.reshape(nz // 2, 8, LANES).astype(BF16)
        sz[layer, :, 1] = odd.reshape(nz // 2, 8, LANES).astype(BF16)
        send_all(
            nz,
            z_peer,
            z,
            lambda t: sz.at[layer, t // 2, lax.rem(t, 2)],
            lambda slot: rz.at[layer, slot],
            y_base + 2,
        )
        total = sz[layer, z // 2, lax.rem(z, 2)].astype(F32)
        wait_all(rz.at[layer, pl.ds(1, nz - 1)], recv_sem.at[y_base + 2])
        for k in range(1, nz):
            total = total + rz[layer, k].astype(F32)
        fresh = xm[layer, z // 2, lax.rem(z, 2)] + total
        az[layer, z // 2, lax.rem(z, 2)] = fresh.astype(BF16)
        mine_z = az.at[layer, z // 2, lax.rem(z, 2)]
        send_all(nz, z_peer, z, lambda t: mine_z, lambda slot: mine_z, y_base + 3)
        wait_all(rz.at[layer, pl.ds(1, nz - 1)], recv_sem.at[y_base + 3])
        parts = list(
            mix(
                az[layer, :, 0].astype(F32).reshape(half, LANES),
                az[layer, :, 1].astype(F32).reshape(half, LANES),
            )
        )

    fx[0] = jnp.where(c == 0, parts[1], parts[0]).astype(BF16)
    swaps[5].start()
    own = jnp.where(c == 0, parts[0], parts[1])
    swaps[5].wait_recv()
    other = fx[1].astype(F32)
    even, odd = mix(jnp.where(c == 0, own, other), jnp.where(c == 0, other, own))
    out = jnp.stack([even.reshape(ny // 2, 8, LANES), odd.reshape(ny // 2, 8, LANES)], axis=1)
    ox[...] = out.reshape(2 * half, LANES).astype(BF16)
    final = pltpu.make_async_copy(ox, out_x, store_sem.at[2])
    final.start()

    swaps[5].wait_send()
    for layer in range(2):
        y_base = 4 * layer
        wait_all(ry.at[layer, pl.ds(1, ny - 1)], send_sem.at[y_base])
        wait_all(ry.at[layer, pl.ds(1, ny - 1), :, pl.ds(0, LANES)], send_sem.at[y_base + 1])
        wait_all(rz.at[layer, pl.ds(1, nz - 1)], send_sem.at[y_base + 2])
        wait_all(rz.at[layer, pl.ds(1, nz - 1)], send_sem.at[y_base + 3])
        pltpu.make_async_copy(nbuf.at[layer], out_s.at[layer], store_sem.at[layer]).wait()
    final.wait()


def per_device(ny, nz, *args):
    stream, states = args[0], args[1]
    anywhere = pl.BlockSpec(memory_space=pl.ANY)
    half = 4 * ny
    model = stream.shape[1] * 2 * ny
    return pl.pallas_call(
        functools.partial(kernel, ny, nz, model),
        out_shape=(
            jax.ShapeDtypeStruct(stream.shape, BF16),
            jax.ShapeDtypeStruct(states.shape, F32),
        ),
        in_specs=[anywhere] * len(args),
        out_specs=(anywhere, anywhere),
        scratch_shapes=[
            pltpu.VMEM((2, *stream.shape), BF16),
            pltpu.VMEM((2, 2, LANES), BF16),
            pltpu.VMEM((2, 2, LANES, 6 * LANES), BF16),
            pltpu.VMEM((2, 2, LANES, LANES), BF16),
            pltpu.VMEM((2, LANES), F32),
            pltpu.VMEM((2, LANES), BF16),
            pltpu.VMEM(states.shape, F32),
            pltpu.VMEM(states.shape, F32),
            pltpu.VMEM((2, ny // 2, 2, 8, 4 * LANES), BF16),
            pltpu.VMEM((2, ny, 8, 4 * LANES), BF16),
            pltpu.VMEM((2, ny // 2, 2, 8, LANES), BF16),
            pltpu.VMEM((2, ny // 2, 2, 8, LANES), F32),
            pltpu.VMEM((2, nz // 2, 2, 8, LANES), BF16),
            pltpu.VMEM((2, nz, 8, LANES), BF16),
            pltpu.VMEM((2, nz // 2, 2, 8, LANES), BF16),
            pltpu.VMEM((2, half, LANES), BF16),
            pltpu.VMEM(stream.shape, BF16),
            pltpu.SemaphoreType.DMA((18,)),
            pltpu.SemaphoreType.DMA((6,)),
            pltpu.SemaphoreType.DMA((6,)),
            pltpu.SemaphoreType.DMA((8,)),
            pltpu.SemaphoreType.DMA((8,)),
            pltpu.SemaphoreType.DMA((3,)),
        ],
        compiler_params=pltpu.CompilerParams(collective_id=0, has_side_effects=True),
    )(*args)


def solution(mesh):
    in_specs = (
        P("grp", "dp"),
        P(None, ("grp", "dp"), "tp", None, None),
        P(None, "dp"),
        P(None, "dp", "tp"),
        P(None, "dp", "tp"),
        P(None, "dp", "tp"),
        P(None, "dp", "tp"),
        P(None, "dp", "tp"),
        P(None, "dp", "tp"),
        P(None, "tp", "dp"),
        P(None, "tp"),
        P(None, "tp"),
    )
    out_specs = (P("grp", "dp"), P(None, ("grp", "dp"), "tp", None, None))
    ny, nz = mesh.shape["dp"] // 2, mesh.shape["tp"]
    return jax.shard_map(
        functools.partial(per_device, ny, nz),
        mesh=mesh,
        in_specs=in_specs,
        out_specs=out_specs,
        check_vma=False,
    )
```

time: 322 us -> 162 us (0.50); the launches traced: 316 us -> 162 us
  Pallas kernels: 0 us -> 158 us
  starting transfers between devices: 104 us -> 0 us
  waiting for transfers between devices: 104 us -> 0 us
  blocking collectives: 88.2 us -> 0 us
  local copies, waits for them, and re-layouts: 9.64 us -> 3.26 us
  other arithmetic: 5.28 us -> 0 us
  matrix products: 4.21 us -> 0 us
    pallas_call x0 -> x1, Pallas kernels: none -> 158 us  [per_device(): pl.pallas_call(functools.partial(kernel, ny, nz, model), out_shape=(jax.S...]
    all_to_all x3 -> x0, starting transfers between devices: 104 us -> none  [the longest x2 98 us: summed_on_arrival(): pieces = lax.all_to_all(in_blocks(x, dim, size), axis, 0, 0, tiled=True)]
    all_to_all x3 -> x0, waiting for transfers between devices: 104 us -> none  [the longest x2 60.3 us: summed_on_arrival(): pieces = lax.all_to_all(in_blocks(x, dim, size), axis, 0, 0, tiled=True)]
    all_to_all x3 -> x0, blocking collectives: 88.2 us -> none  [from_everyone(): return lax.all_to_all(copies, axis, split_axis=0, concat_axis=0, tiled=True)]
    dot_general x18 -> x0, matrix products: 4.21 us -> none  [the longest x12 1.58 us: run_block(): jnp.dot(normed, weight, preferred_element_type=jnp.float32)]
  transfers between devices with their start and end apart: 3 -> 0, of which waited for: 3 -> 0; matrix products, arithmetic and copies ran while one was open for 0% -> 0% of each run, Pallas kernels for 0% -> 0%
where the time goes in v1:
time: 162 us
  Pallas kernels  158 us (98%)
  local copies, waits for them, and re-layouts  3.26 us (2%)
    pallas_call x1, Pallas kernels, per_device(): pl.pallas_call(functools.partial(kernel, ny, nz, model), out_shape=(jax.S...  158 us
    unnamed x2, local copies, waits for them, and re-layouts  3.26 us

profile of v1, /device:TPU:5, one launch (start us, length us, event | category | flops | bytes accessed | tf_op | source)
XLA Modules:
  0.0 161.9 jit_solution(14333085505273272848)
XLA Ops:
  0.6 158.0 %shard_map.131 = (bf16[128,128]{1,0:T(8,128)(2,1)}, f32[2,4,2,64,64]{4,3,2,1,0:T(8,128)}) custom-call(bf16[128,128]{1,0:T(8,128)(2,1)} %stream.1, f32[2,4,2,64,64]{4,3,2,1,0:T(8,128)} %states.1, bf16[2,128]{1,0:T(2,128)(2,1)} %gain.1, bf16[2,128,128]{2,1,0:T(8,128)(2,1)} %w0.1, bf16[2,128,128]{2,1,0:T(8,128)(2,1)} %w1.1, bf16[2,128,128]{2,1,0:T(8,128)(2,1)} %w2.1, ...), custom_call_target="tpu_custom_call" | custom-call | tf_op jit(solution)/shard_map/pallas_call | solution.py:361
  158.6 1.4 copy.16
  160.0 1.9 %copy.17 = f32[2,4,2,64,64]{4,3,2,1,0:T(8,128)} copy(f32[2,4,2,64,64]{4,3,2,1,0:T(8,128)} %get-tuple-element.5) | data formatting | bytes 524288

commit v2 on v1

--- a/solution.py
+++ b/solution.py
@@ -32,6 +32,10 @@
     s0 = jnp.sum(jnp.where(first, t, 0.0), axis=1, keepdims=True)
     s1 = jnp.sum(jnp.where(first, 0.0, t), axis=1, keepdims=True)
     return jnp.where(first, s0, s1)
+
+
+def owners_of(nz):
+    return min(4, nz // 2)
 
 
 def sigmoid(t):
@@ -63,7 +67,6 @@
     bbuf,
     hbuf,
     sbuf,
-    nbuf,
     sy,
     ry,
     my,
@@ -72,19 +75,20 @@
     rz,
     az,
     fx,
-    ox,
     load_sem,
     part_send,
     part_recv,
     send_sem,
     recv_sem,
-    store_sem,
 ):
     z = lax.axis_index("tp")
     d = lax.axis_index("dp")
     y = d // 2
     c = lax.rem(d, 2)
     half = 4 * ny
+    owners = owners_of(nz)
+    step = nz // owners
+    mine = lax.rem(z, step)
 
     def y_peer(k):
         return {"dp": lax.rem(y + k, ny) * 2 + c}
@@ -142,7 +146,6 @@
         exchange(wbuf.at[0, c], wbuf.at[0, c], 2),
         exchange(obuf.at[c], obuf.at[c], 3),
         exchange(wbuf.at[1, c], wbuf.at[1, c], 4),
-        exchange(fx.at[0], fx.at[1], 5),
     ]
 
     def send_all(n, peer, here, src, dst, k):
@@ -165,6 +168,33 @@
     def wait_all(ref, sem):
         pltpu.make_async_copy(ref, ref, sem).wait()
 
+    def put_pieces(buf, layer, even, odd):
+        for i in range(step // 2):
+            for lane, part in enumerate((even, odd)):
+                blocks = part.reshape(owners, step // 2, 8, LANES)[:, i]
+                buf[layer, 2 * i + lane] = blocks.astype(buf.dtype)
+
+    def take_pieces(pieces):
+        pairs = []
+        for lane in range(2):
+            picked = [pieces[2 * i + lane] for i in range(step // 2)]
+            pairs.append(jnp.stack(picked, axis=1).reshape(half, LANES))
+        return mix(pairs[0], pairs[1])
+
+    def spread(ref, k, cores):
+        for off in sorted(range(1 - step // 2, step // 2 + 1), key=lambda t: -abs(t)):
+            for core in cores:
+                if off == 0 and core is c:
+                    continue
+                pltpu.make_async_remote_copy(
+                    src_ref=ref,
+                    dst_ref=ref,
+                    send_sem=send_sem.at[k],
+                    recv_sem=recv_sem.at[k],
+                    device_id={"tp": lax.rem(z + off + nz, nz), "dp": 2 * y + core},
+                    device_id_type=MESH,
+                ).start()
+
     loads["x"].wait()
     loads["g"].wait()
     for r in range(6):
@@ -189,8 +219,7 @@
     for layer in range(2):
         y_base = 4 * layer
         even, odd = mix(parts[0], parts[1])
-        xm[layer, :, 0] = even.reshape(ny // 2, 8, LANES)
-        xm[layer, :, 1] = odd.reshape(ny // 2, 8, LANES)
+        put_pieces(xm, layer, even, odd)
 
         normed = jnp.concatenate(
             [parts[core] * gbuf[core, layer : layer + 1].astype(F32) for core in range(2)], axis=1
@@ -288,13 +317,11 @@
             lanes = slice(h * HEAD, (h + 1) * HEAD)
             dec_h, kr_h, key_h = decay[:, lanes], key_rate[:, lanes], key_vec[:, lanes]
             for s in range(4):
-                nbuf[layer, s, h] = (
+                out_s[layer, s, h] = (
                     sbuf[layer, s, h] * dec_h[s : s + 1]
                     - removed_t[lanes, s : s + 1] * kr_h[s : s + 1]
                     + value_t[lanes, s : s + 1] * key_h[s : s + 1]
                 )
-        store = pltpu.make_async_copy(nbuf.at[layer], out_s.at[layer], store_sem.at[layer])
-        store.start()
 
         if layer == 0:
             swaps[3].wait()
@@ -305,67 +332,73 @@
             jnp.dot(mixed, obuf[0, layer], preferred_element_type=F32),
             jnp.dot(mixed, obuf[1, layer], preferred_element_type=F32),
         )
-        sz[layer, :, 0] = even.reshape(nz // 2, 8, LANES).astype(BF16)
-        sz[layer, :, 1] = odd.reshape(nz // 2, 8, LANES).astype(BF16)
+        put_pieces(sz, layer, even, odd)
         send_all(
             nz,
             z_peer,
             z,
-            lambda t: sz.at[layer, t // 2, lax.rem(t, 2)],
+            lambda t: sz.at[layer, lax.rem(t, step)],
             lambda slot: rz.at[layer, slot],
             y_base + 2,
         )
-        total = sz[layer, z // 2, lax.rem(z, 2)].astype(F32)
+        total = sz[layer, mine].astype(F32)
         wait_all(rz.at[layer, pl.ds(1, nz - 1)], recv_sem.at[y_base + 2])
         for k in range(1, nz):
             total = total + rz[layer, k].astype(F32)
-        fresh = xm[layer, z // 2, lax.rem(z, 2)] + total
-        az[layer, z // 2, lax.rem(z, 2)] = fresh.astype(BF16)
-        mine_z = az.at[layer, z // 2, lax.rem(z, 2)]
-        send_all(nz, z_peer, z, lambda t: mine_z, lambda slot: mine_z, y_base + 3)
-        wait_all(rz.at[layer, pl.ds(1, nz - 1)], recv_sem.at[y_base + 3])
-        parts = list(
-            mix(
-                az[layer, :, 0].astype(F32).reshape(half, LANES),
-                az[layer, :, 1].astype(F32).reshape(half, LANES),
-            )
-        )
-
-    fx[0] = jnp.where(c == 0, parts[1], parts[0]).astype(BF16)
-    swaps[5].start()
-    own = jnp.where(c == 0, parts[0], parts[1])
-    swaps[5].wait_recv()
-    other = fx[1].astype(F32)
-    even, odd = mix(jnp.where(c == 0, own, other), jnp.where(c == 0, other, own))
+        fresh = (xm[layer, mine] + total).astype(BF16)
+        if layer == 0:
+            az[mine] = fresh
+            spread(az.at[mine], y_base + 3, (c,))
+            wait_all(az.at[pl.ds(0, step - 1)], recv_sem.at[y_base + 3])
+            parts = list(take_pieces(az[...].astype(F32)))
+        else:
+            fx[c * step + mine] = fresh
+            spread(fx.at[c * step + mine], y_base + 3, (c, 1 - c))
+            wait_all(fx.at[pl.ds(0, 2 * step - 1)], recv_sem.at[y_base + 3])
+
+    halves = []
+    for core in range(2):
+        a, b = take_pieces(fx[core * step : (core + 1) * step].astype(F32))
+        halves.append(jnp.where(c == 0, a, b))
+    even, odd = mix(halves[0], halves[1])
     out = jnp.stack([even.reshape(ny // 2, 8, LANES), odd.reshape(ny // 2, 8, LANES)], axis=1)
-    ox[...] = out.reshape(2 * half, LANES).astype(BF16)
-    final = pltpu.make_async_copy(ox, out_x, store_sem.at[2])
-    final.start()
-
-    swaps[5].wait_send()
+    out_x[...] = out.reshape(2 * half, LANES).astype(BF16)
+
     for layer in range(2):
         y_base = 4 * layer
         wait_all(ry.at[layer, pl.ds(1, ny - 1)], send_sem.at[y_base])
         wait_all(ry.at[layer, pl.ds(1, ny - 1), :, pl.ds(0, LANES)], send_sem.at[y_base + 1])
         wait_all(rz.at[layer, pl.ds(1, nz - 1)], send_sem.at[y_base + 2])
-        wait_all(rz.at[layer, pl.ds(1, nz - 1)], send_sem.at[y_base + 3])
-        pltpu.make_async_copy(nbuf.at[layer], out_s.at[layer], store_sem.at[layer]).wait()
-    final.wait()
+        spread_wait = az.at[pl.ds(0, step - 1)] if layer == 0 else fx.at[pl.ds(0, 2 * step - 1)]
+        wait_all(spread_wait, send_sem.at[y_base + 3])
+
+
+def write_out(x, s, out_x, out_s, sem):
+    copies = [
+        pltpu.make_async_copy(x, out_x, sem.at[0]),
+        pltpu.make_async_copy(s.at[0], out_s.at[0], sem.at[1]),
+        pltpu.make_async_copy(s.at[1], out_s.at[1], sem.at[2]),
+    ]
+    for copy in copies:
+        copy.start()
+    for copy in copies:
+        copy.wait()
 
 
 def per_device(ny, nz, *args):
     stream, states = args[0], args[1]
     anywhere = pl.BlockSpec(memory_space=pl.ANY)
-    half = 4 * ny
+    owners = owners_of(nz)
+    pieces = (nz // owners, owners, 8, LANES)
     model = stream.shape[1] * 2 * ny
-    return pl.pallas_call(
+    results = pl.pallas_call(
         functools.partial(kernel, ny, nz, model),
         out_shape=(
-            jax.ShapeDtypeStruct(stream.shape, BF16),
-            jax.ShapeDtypeStruct(states.shape, F32),
+            pltpu.VMEM(stream.shape, BF16),
+            pltpu.VMEM(states.shape, F32),
         ),
         in_specs=[anywhere] * len(args),
-        out_specs=(anywhere, anywhere),
+        out_specs=(pl.BlockSpec(memory_space=pltpu.VMEM),) * 2,
         scratch_shapes=[
             pltpu.VMEM((2, *stream.shape), BF16),
             pltpu.VMEM((2, 2, LANES), BF16),
@@ -374,25 +407,33 @@
             pltpu.VMEM((2, LANES), F32),
             pltpu.VMEM((2, LANES), BF16),
             pltpu.VMEM(states.shape, F32),
-            pltpu.VMEM(states.shape, F32),
             pltpu.VMEM((2, ny // 2, 2, 8, 4 * LANES), BF16),
             pltpu.VMEM((2, ny, 8, 4 * LANES), BF16),
             pltpu.VMEM((2, ny // 2, 2, 8, LANES), BF16),
-            pltpu.VMEM((2, ny // 2, 2, 8, LANES), F32),
-            pltpu.VMEM((2, nz // 2, 2, 8, LANES), BF16),
-            pltpu.VMEM((2, nz, 8, LANES), BF16),
-            pltpu.VMEM((2, nz // 2, 2, 8, LANES), BF16),
-            pltpu.VMEM((2, half, LANES), BF16),
-            pltpu.VMEM(stream.shape, BF16),
+            pltpu.VMEM((2, *pieces), F32),
+            pltpu.VMEM((2, *pieces), BF16),
+            pltpu.VMEM((2, nz, *pieces[1:]), BF16),
+            pltpu.VMEM(pieces, BF16),
+            pltpu.VMEM((2 * pieces[0], *pieces[1:]), BF16),
             pltpu.SemaphoreType.DMA((18,)),
-            pltpu.SemaphoreType.DMA((6,)),
-            pltpu.SemaphoreType.DMA((6,)),
+            pltpu.SemaphoreType.DMA((5,)),
+            pltpu.SemaphoreType.DMA((5,)),
             pltpu.SemaphoreType.DMA((8,)),
             pltpu.SemaphoreType.DMA((8,)),
-            pltpu.SemaphoreType.DMA((3,)),
         ],
         compiler_params=pltpu.CompilerParams(collective_id=0, has_side_effects=True),
     )(*args)
+    inside = pl.BlockSpec(memory_space=pltpu.VMEM)
+    return pl.pallas_call(
+        write_out,
+        out_shape=(
+            jax.ShapeDtypeStruct(stream.shape, BF16),
+            jax.ShapeDtypeStruct(states.shape, F32),
+        ),
+        in_specs=[inside, inside],
+        out_specs=(anywhere, anywhere),
+        scratch_shapes=[pltpu.SemaphoreType.DMA((3,))],
+    )(*(pltpu.with_memory_space_constraint(r, pltpu.VMEM) for r in results))
 
 
 def solution(mesh):

time: 162 us -> 153 us (0.944)
  Pallas kernels: 158 us -> 152 us
  local copies, waits for them, and re-layouts: 3.26 us -> 0 us
    pallas_call x1 -> x2, Pallas kernels: 158 us -> 152 us  [the longest x1 151 us: per_device(): pl.pallas_call(functools.partial(kernel, ny, nz, model), out_shape=(pltpu...]
    unnamed x2 -> x0, local copies, waits for them, and re-layouts: 3.26 us -> none
where the time goes in v2:
time: 153 us
  Pallas kernels  152 us (99%)
    pallas_call x1, Pallas kernels, per_device(): pl.pallas_call(functools.partial(kernel, ny, nz, model), out_shape=(pltpu...  151 us

profile of v2, /device:TPU:5, one launch (start us, length us, event | category | flops | bytes accessed | tf_op | source)
XLA Modules:
  0.0 152.7 jit_solution(899004323986028167)
XLA Ops:
  0.6 151.2 %shard_map.131 = (bf16[128,128]{1,0:T(8,128)(2,1)S(1)}, f32[2,4,2,64,64]{4,3,2,1,0:T(8,128)S(1)}) custom-call(bf16[128,128]{1,0:T(8,128)(2,1)} %stream.1, f32[2,4,2,64,64]{4,3,2,1,0:T(8,128)} %states.1, bf16[2,128]{1,0:T(2,128)(2,1)} %gain.1, bf16[2,128,128]{2,1,0:T(8,128)(2,1)} %w0.1, bf16[2,128,128]{2,1,0:T(8,128)(2,1)} %w1.1, bf16[2,128,128]{2,1,0:T(8,128)(2,1)} %w2.1, ...), custom_call_target="tpu_custom_call" | custom-call | tf_op jit(solution)/shard_map/pallas_call | solution.py:394
  151.9 0.8 shard_map.132
